TPU v7x, 32 devices: a whole 2x2x4 slice. The times are simulated.
32 devices in a mesh: grp: 2 (over y), fs: 4 (over z), tp: 4 (over x, core).
Axes of the slice: x: 2, y: 2, z: 4, core: 2. Of those that a mesh axis runs over, the one named last changes fastest.
Arguments:
- tokens: bfloat16 [1024, 2048], P(('grp', 'fs')), parts along dimension 0, may hold values from -12 to 12, as said below
- mix_heads: bfloat16 [1024, 2048], P(('grp', 'fs'), 'tp'), parts along dimension 0, may hold values from -6 to 6
- norm_first: float32 [2048], replicated, may hold values from 0.1 to 1.9
- gate_first: bfloat16 [2048, 5632], P('fs', 'tp'), may hold values from -0.125 to 0.125
- up_first: bfloat16 [2048, 5632], P('fs', 'tp'), may hold values from -0.125 to 0.125
- down_first: bfloat16 [5632, 2048], P('tp', 'fs'), may hold values from -0.078125 to 0.078125
- out_weight: bfloat16 [2048, 2048], P('tp', 'fs'), may hold values from -0.125 to 0.125
- norm_second: float32 [2048], replicated, may hold values from 0.1 to 1.9
- gate_second: bfloat16 [2048, 5632], P('fs', 'tp'), may hold values from -0.125 to 0.125
- up_second: bfloat16 [2048, 5632], P('fs', 'tp'), may hold values from -0.125 to 0.125
- down_second: bfloat16 [5632, 2048], P('tp', 'fs'), may hold values from -0.078125 to 0.078125
Outputs:
- layer_out: bfloat16 [1024, 2048], P(('grp', 'fs')), parts along dimension 0
There are 2 independent parts, one for each index of `grp`. A program takes and returns all parts, laid end to end along the dimension named above; an argument that names none is the same for every part. Nothing has to cross between parts.
Inputs may be any that keep to these rules, and one draw needn't show every extreme that they name: Each row of tokens carries a scale of its own.
All inputs are finite; a program needn't handle non-finite values.
Results may differ from a plain program's by a relative error of at most 0.014.
Values may be sent and summed in bfloat16 or wider, within the bound.
A program may use at most 64 MiB of HBM per device.

v0:
```python
import jax
import jax.numpy as jnp
from jax import lax
from jax.sharding import PartitionSpec as P

EPS = 0.1


def norm_rows(row_block, gain_vector):
    widened = row_block.astype(jnp.float32)
    scaled = widened * lax.rsqrt(jnp.mean(widened * widened, axis=-1, keepdims=True) + EPS)
    return (scaled * gain_vector).astype(jnp.bfloat16)


def gate_values(normed, gate_weight, value_weight):
    whole_gate, whole_values = (
        lax.all_gather(gate_weight, "fs", axis=0, tiled=True),
        lax.all_gather(value_weight, "fs", axis=0, tiled=True),
    )
    return (
        jnp.dot(normed, whole_gate, preferred_element_type=jnp.float32),
        jnp.dot(normed, whole_values, preferred_element_type=jnp.float32),
    )


def half_branch(normed, gate_weight, value_weight, down_weight):
    gates, values = gate_values(normed, gate_weight, value_weight)
    hidden = (jax.nn.silu(gates) * values).astype(jnp.bfloat16)
    return 0.5 * jnp.dot(
        hidden,
        lax.all_gather(down_weight, "fs", axis=1, tiled=True),
        preferred_element_type=jnp.float32,
    )


def share_sum(block_terms):
    return lax.psum_scatter(
        block_terms.astype(jnp.bfloat16), "tp", scatter_dimension=0, tiled=True
    ).astype(jnp.float32)


def join_rows(row_block):
    return lax.all_gather(row_block, "tp", axis=0, tiled=True)


def local(
    tokens,
    mix_heads,
    norm_first,
    gate_first,
    up_first,
    down_first,
    out_weight,
    norm_second,
    gate_second,
    up_second,
    down_second,
):
    normed_one = norm_rows(tokens, norm_first)
    first_terms = half_branch(normed_one, gate_first, up_first, down_first)
    heads_out = jnp.dot(
        mix_heads,
        lax.all_gather(out_weight, "fs", axis=1, tiled=True),
        preferred_element_type=jnp.float32,
    )
    first_terms = first_terms + heads_out
    share_rows = tokens.shape[0] // lax.axis_size("tp")
    offset = lax.axis_index("tp") * share_rows
    own_rows = lax.dynamic_slice_in_dim(tokens, offset, share_rows, 0).astype(jnp.float32)
    resid_two = own_rows + share_sum(first_terms)
    normed_two = join_rows(norm_rows(resid_two, norm_second))
    second_terms = half_branch(normed_two, gate_second, up_second, down_second)
    finished = (resid_two + share_sum(second_terms)).astype(jnp.bfloat16)
    return join_rows(finished)


def solution(mesh):
    in_specs = (
        P(("grp", "fs"), None),
        P(("grp", "fs"), "tp"),
        P(),
        P("fs", "tp"),
        P("fs", "tp"),
        P("tp", "fs"),
        P("tp", "fs"),
        P(),
        P("fs", "tp"),
        P("fs", "tp"),
        P("tp", "fs"),
    )
    out_specs = P(("grp", "fs"), None)
    return jax.shard_map(local, mesh=mesh, in_specs=in_specs, out_specs=out_specs, check_vma=False)
```

profile of v0, /device:TPU:0, one launch (start us, length us, event | category | flops | bytes accessed | tf_op | source)
XLA Modules:
  0.0 763.6 jit_solution(13067139635178607233)
XLA Ops:
  6.5 0.0 copy-start
  6.5 0.0 all-gather.8.cloned.1.call-start
  6.5 0.7 all-gather.8.cloned.1.call-update
  7.3 0.0 copy-start.1
  7.3 0.0 copy-start.3
  7.3 0.0 all-gather.10.cloned.1.call-start
  7.3 0.7 all-gather.10.cloned.1.call-update
  8.0 0.0 all-gather.12.cloned.1.call-start
  8.1 0.7 all-gather.12.cloned.1.call-update
  8.8 0.0 all-gather.14.cloned.1.call-start
  8.8 0.5 all-gather.14.cloned.1.call-update
  9.3 0.0 reduce-scatter.3.cloned.1.call-start
  9.4 1.2 fusion.4
  10.6 107.7 %all-gather.8.cloned.1.call-done = bf16[2048,1408]{1,0:T(8,128)(2,1)} async-done(((bf16[512,1408]{1,0:T(8,128)(2,1)}), bf16[2048,1408]{1,0:T(8,128)(2,1)}) %all-gather.8.cloned.1.call-update) | async-done | bytes 5767184 | tf_op jit(solution)/shard_map/all_gather | solution.py:17
  118.3 3.9 fusion.11
  122.2 102.7 %all-gather.10.cloned.1.call-done = bf16[2048,1408]{1,0:T(8,128)(2,1)} async-done(((bf16[512,1408]{1,0:T(8,128)(2,1)}), bf16[2048,1408]{1,0:T(8,128)(2,1)}) %all-gather.10.cloned.1.call-update) | async-done | bytes 5767184 | tf_op jit(solution)/shard_map/all_gather | solution.py:18
  224.9 106.5 %all-gather.12.cloned.1.call-done = bf16[1408,2048]{1,0:T(8,128)(2,1)} async-done(((bf16[1408,512]{1,0:T(8,128)(2,1)}), bf16[1408,2048]{1,0:T(8,128)(2,1)}) %all-gather.12.cloned.1.call-update) | async-done | bytes 5767184 | tf_op jit(solution)/shard_map/all_gather | solution.py:31
  331.5 0.0 copy-done.1
  331.5 0.0 copy-done.3
  331.5 6.3 convolution_multiply_fusion.3
  337.8 0.0 copy-start.4
  337.8 39.1 %all-gather.14.cloned.1.call-done = bf16[512,2048]{1,0:T(8,128)(2,1)} async-done(((bf16[512,512]{1,0:T(8,128)(2,1)}), bf16[512,2048]{1,0:T(8,128)(2,1)}) %all-gather.14.cloned.1.call-update) | async-done | bytes 2097168 | tf_op jit(solution)/shard_map/all_gather | solution.py:63
  376.8 0.0 copy-done
  376.8 2.8 fusion
  379.7 0.0 reduce-scatter.3.cloned.1.call-update
  379.7 0.0 all-gather.16.cloned.1.call-start
  379.8 0.5 all-gather.16.cloned.1.call-update
  380.3 0.0 all-gather.18.cloned.1.call-start
  380.3 0.7 all-gather.18.cloned.1.call-update
  381.0 0.0 all-gather.20.cloned.1.call-start
  381.1 0.7 all-gather.20.cloned.1.call-update
  381.8 0.0 reduce-scatter.5.cloned.1.call-start
  381.8 18.5 %reduce-scatter.3.cloned.1.call-done = bf16[32,2048]{1,0:T(8,128)(2,1)} async-done(((bf16[128,2048]{1,0:T(8,128)(2,1)}), bf16[32,2048]{1,0:T(8,128)(2,1)}) %reduce-scatter.3.cloned.1.call-update) | async-done | bytes 131088 | tf_op jit(solution)/shard_map/reduce_scatter | solution.py:37
  400.3 1.1 multiply_reduce_fusion
  401.4 0.0 copy-done.4
  401.4 1.0 multiply_convert_fusion
  402.4 6.6 all_gather.31
  409.0 99.5 %all-gather.16.cloned.1.call-done = bf16[2048,1408]{1,0:T(8,128)(2,1)} async-done(((bf16[512,1408]{1,0:T(8,128)(2,1)}), bf16[2048,1408]{1,0:T(8,128)(2,1)}) %all-gather.16.cloned.1.call-update) | async-done | bytes 5767184 | tf_op jit(solution)/shard_map/all_gather | solution.py:17
  508.5 3.6 fusion.15
  512.1 0.0 copy-start.2
  512.1 102.9 %all-gather.18.cloned.1.call-done = bf16[2048,1408]{1,0:T(8,128)(2,1)} async-done(((bf16[512,1408]{1,0:T(8,128)(2,1)}), bf16[2048,1408]{1,0:T(8,128)(2,1)}) %all-gather.18.cloned.1.call-update) | async-done | bytes 5767184 | tf_op jit(solution)/shard_map/all_gather | solution.py:18
  615.0 106.5 %all-gather.20.cloned.1.call-done = bf16[1408,2048]{1,0:T(8,128)(2,1)} async-done(((bf16[1408,512]{1,0:T(8,128)(2,1)}), bf16[1408,2048]{1,0:T(8,128)(2,1)}) %all-gather.20.cloned.1.call-update) | async-done | bytes 5767184 | tf_op jit(solution)/shard_map/all_gather | solution.py:31
  721.6 7.1 fusion.1
  728.6 0.0 reduce-scatter.5.cloned.1.call-update
  728.6 20.0 %reduce-scatter.5.cloned.1.call-done = bf16[32,2048]{1,0:T(8,128)(2,1)} async-done(((bf16[128,2048]{1,0:T(8,128)(2,1)}), bf16[32,2048]{1,0:T(8,128)(2,1)}) %reduce-scatter.5.cloned.1.call-update) | async-done | bytes 131088 | tf_op jit(solution)/shard_map/reduce_scatter | solution.py:37
  748.7 1.0 add_convert_fusion
  749.7 6.6 all_gather.35
  756.3 0.8 copy.13
  (3 shorter events, 0.0 us)
Async XLA Ops:
  6.5 370.3 %copy-start = (bf16[128,512]{1,0:T(8,128)(2,1)S(1)}, bf16[128,512]{1,0:T(8,128)(2,1)}, u32[]{:S(2)}) copy-start(bf16[128,512]{1,0:T(8,128)(2,1)} %param.12) | copy-start | bytes 393220
  6.5 111.8 %all-gather.8.cloned.1.call-start = ((), (), s32[]{:S(2)}) async-start(), calls=%async_computation.2 | async-start | bytes 7208960 | tf_op jit(solution)/shard_map/all_gather | solution.py:17
  7.3 324.2 %copy-start.1 = (bf16[128,2048]{1,0:T(8,128)(2,1)S(1)}, bf16[128,2048]{1,0:T(8,128)(2,1)}, u32[]{:S(2)}) copy-start(bf16[128,2048]{1,0:T(8,128)(2,1)} %param.11) | copy-start | bytes 1572868
  7.3 324.2 %copy-start.3 = (f32[2048]{0:T(1024)S(1)}, f32[2048]{0:T(1024)}, u32[]{:S(2)}) copy-start(f32[2048]{0:T(1024)} %param.13) | copy-start | bytes 24580
  7.3 217.6 %all-gather.10.cloned.1.call-start = ((), (), s32[]{:S(2)}) async-start(), calls=%async_computation.3 | async-start | bytes 7208960 | tf_op jit(solution)/shard_map/all_gather | solution.py:18
  8.0 323.4 %all-gather.12.cloned.1.call-start = ((), (), s32[]{:S(2)}) async-start(), calls=%async_computation.4 | async-start | bytes 7208960 | tf_op jit(solution)/shard_map/all_gather | solution.py:31
  8.8 368.1 %all-gather.14.cloned.1.call-start = ((), (), s32[]{:S(2)}) async-start(), calls=%async_computation.5 | async-start | bytes 2621440 | tf_op jit(solution)/shard_map/all_gather | solution.py:63
  9.3 391.0 %reduce-scatter.3.cloned.1.call-start = ((), (), s32[]{:S(2)}) async-start(), calls=%async_computation.6 | async-start | bytes 655360 | tf_op jit(solution)/shard_map/reduce_scatter | solution.py:37
  337.8 63.6 %copy-start.4 = (f32[2048]{0:T(1024)S(1)}, f32[2048]{0:T(1024)}, u32[]{:S(2)}) copy-start(f32[2048]{0:T(1024)} %param.18) | copy-start | bytes 24580
  379.7 128.8 %all-gather.16.cloned.1.call-start = ((), (), s32[]{:S(2)}) async-start(), calls=%async_computation.7 | async-start | bytes 7208960 | tf_op jit(solution)/shard_map/all_gather | solution.py:17
  380.3 234.7 %all-gather.18.cloned.1.call-start = ((), (), s32[]{:S(2)}) async-start(), calls=%async_computation.8 | async-start | bytes 7208960 | tf_op jit(solution)/shard_map/all_gather | solution.py:18
  381.0 340.5 %all-gather.20.cloned.1.call-start = ((), (), s32[]{:S(2)}) async-start(), calls=%async_computation.9 | async-start | bytes 7208960 | tf_op jit(solution)/shard_map/all_gather | solution.py:31
  381.8 366.9 %reduce-scatter.5.cloned.1.call-start = ((), (), s32[]{:S(2)}) async-start(), calls=%async_computation.10 | async-start | bytes 655360 | tf_op jit(solution)/shard_map/reduce_scatter | solution.py:37
  512.1 236.6 %copy-start.2 = (bf16[32,2048]{1,0:T(8,128)(2,1)S(1)}, bf16[32,2048]{1,0:T(8,128)(2,1)}, u32[]{:S(2)}) copy-start(bf16[32,2048]{1,0:T(8,128)(2,1)} %reduce-scatter.3.cloned.1.call-done) | copy-start | bytes 393220
Sparse Core Ops, SparseCore 0:
  8.9 109.3 all-gather.7
  119.9 104.9 all-gather.9
  226.5 104.9 all-gather.11
  332.9 43.9 all-gather.13
  379.8 20.4 reduce-scatter.2
  401.7 106.6 all-gather.15
  510.0 104.9 all-gather.17
  616.6 104.9 all-gather.19
  728.8 19.8 reduce-scatter.4
where the time goes:
time: 764 us
  waiting for transfers between devices  708 us (93%)
  matrix products  23.7 us (3%)
  between operations  13.3 us (2%)
  blocking collectives  13.2 us (2%)
    all_gather x2, waiting for transfers between devices, half_branch(): lax.all_gather(down_weight, 'fs', axis=1, tiled=True)  213 us
    all_gather x2, waiting for transfers between devices, gate_values(): lax.all_gather(gate_weight, 'fs', axis=0, tiled=True)  207 us
    all_gather x2, waiting for transfers between devices, gate_values(): lax.all_gather(value_weight, 'fs', axis=0, tiled=True)  206 us
    all_gather x1, waiting for transfers between devices, local(): lax.all_gather(out_weight, 'fs', axis=1, tiled=True)  39.1 us
    reduce_scatter x2, waiting for transfers between devices, share_sum(): lax.psum_scatter(block_terms.astype(jnp.bfloat16), 'tp', scatter_dimensio...  38.5 us
  transfers between devices with their start and end apart: 9, of which 9 were waited for; matrix products, arithmetic and copies ran while one was open for 2% of the time, Pallas kernels for 0%

commit v1 on v0

--- a/solution.py
+++ b/solution.py
@@ -4,6 +4,27 @@
 from jax.sharding import PartitionSpec as P
 
 EPS = 0.1
+
+
+def ring_gather(x, axis, dim):
+    length, position, width = (lax.axis_size(axis), lax.axis_index(axis), x.shape[dim])
+    right = [(i, (i + 1) % length) for i in range(length)]
+    downward = [(i, (i - 1) % length) for i in range(length)]
+    whole = jnp.zeros((*x.shape[:dim], length * width, *x.shape[dim + 1 :]), x.dtype)
+    whole = lax.dynamic_update_slice_in_dim(whole, x, position * width, axis=dim)
+    from_left = from_right = x
+    half = length // 2
+    for step in range(1, half + 1):
+        from_left = lax.ppermute(from_left, axis, right)
+        whole = lax.dynamic_update_slice_in_dim(
+            whole, from_left, (position - step) % length * width, axis=dim
+        )
+        if step < length - half:
+            from_right = lax.ppermute(from_right, axis, downward)
+            whole = lax.dynamic_update_slice_in_dim(
+                whole, from_right, (position + step) % length * width, axis=dim
+            )
+    return whole
 
 
 def norm_rows(row_block, gain_vector):
@@ -27,9 +48,7 @@
     gates, values = gate_values(normed, gate_weight, value_weight)
     hidden = (jax.nn.silu(gates) * values).astype(jnp.bfloat16)
     return 0.5 * jnp.dot(
-        hidden,
-        lax.all_gather(down_weight, "fs", axis=1, tiled=True),
-        preferred_element_type=jnp.float32,
+        hidden, ring_gather(down_weight, "fs", 1), preferred_element_type=jnp.float32
     )
 
 

time: 764 us -> 690 us (0.903)
  waiting for transfers between devices: 708 us -> 575 us
  starting transfers between devices: 0.31 us -> 35.8 us
  local copies, waits for them, and re-layouts: 0.82 us -> 22.6 us
    ppermute x0 -> x6, waiting for transfers between devices: none -> 273 us  [the longest x4 158 us: ring_gather(): from_left = lax.ppermute(from_left, axis, right)]
    all_gather x2 -> x0, waiting for transfers between devices: 213 us -> none  [half_branch(): lax.all_gather(down_weight, 'fs', axis=1, tiled=True)]
    all_gather x2, waiting for transfers between devices: 207 us -> 70.9 us  [gate_values(): lax.all_gather(gate_weight, 'fs', axis=0, tiled=True)]
    all_gather x1, waiting for transfers between devices: 39.1 us -> 0.01 us  [local(): lax.all_gather(out_weight, 'fs', axis=1, tiled=True)]
    ppermute x0 -> x6, starting transfers between devices: none -> 35.6 us  [the longest x4 29.7 us: ring_gather(): from_left = lax.ppermute(from_left, axis, right)]
    reduce_scatter x2, waiting for transfers between devices: 38.5 us -> 20 us  [share_sum(): lax.psum_scatter(block_terms.astype(jnp.bfloat16), 'tp', scatter_dimensio...]
    dynamic_update_slice x0 -> x8, local copies, waits for them, and re-layouts: none -> 15.4 us  [the longest x4 7.71 us: ring_gather(): lax.dynamic_update_slice_in_dim(whole, from_left, (position - step) % len...]
  transfers between devices with their start and end apart: 9 -> 13, of which waited for: 9 -> 11; matrix products, arithmetic and copies ran while one was open for 2% -> 5% of each run, Pallas kernels for 0% -> 0%
where the time goes in v1:
time: 690 us; the launch traced here: 689 us
  waiting for transfers between devices  575 us (83%)
  starting transfers between devices  35.8 us (5%)
  matrix products  24.5 us (4%)
  local copies, waits for them, and re-layouts  22.6 us (3%)
  blocking collectives  13.8 us (2%)
  between operations  13.6 us (2%)
    all_gather x2, waiting for transfers between devices, gate_values(): lax.all_gather(value_weight, 'fs', axis=0, tiled=True)  207 us
    ppermute x4, waiting for transfers between devices, ring_gather(): from_left = lax.ppermute(from_left, axis, right)  158 us
    ppermute x2, waiting for transfers between devices, ring_gather(): from_right = lax.ppermute(from_right, axis, downward)  116 us
    all_gather x2, waiting for transfers between devices, gate_values(): lax.all_gather(gate_weight, 'fs', axis=0, tiled=True)  70.9 us
    ppermute x4, starting transfers between devices, ring_gather(): from_left = lax.ppermute(from_left, axis, right)  29.7 us
    reduce_scatter x2, waiting for transfers between devices, share_sum(): lax.psum_scatter(block_terms.astype(jnp.bfloat16), 'tp', scatter_dimensio...  20 us
    dot_general x2, matrix products, half_branch(): jnp.dot(hidden, ring_gather(down_weight, 'fs', 1), preferred_element_type...  14.3 us
  transfers between devices with their start and end apart: 13, of which 11 were waited for; matrix products, arithmetic and copies ran while one was open for 5% of the time, Pallas kernels for 0%

profile of v1, /device:TPU:0, one launch (start us, length us, event | category | flops | bytes accessed | tf_op | source)
XLA Modules:
  0.0 689.4 jit_solution(4010602772304346363)
XLA Ops:
  6.5 0.7 all-gather.10.cloned.1.call-update
  7.3 0.0 all-gather.6.cloned.1.call-start
  7.3 0.7 all-gather.6.cloned.1.call-update
  8.0 0.0 all-gather.8.cloned.1.call-start
  8.1 0.7 all-gather.8.cloned.1.call-update
  8.7 0.0 reduce-scatter.3.cloned.1.call-start
  8.8 3.1 collective-permute-start
  11.9 2.1 collective-permute-start.1
  14.0 55.3 %collective-permute-done = bf16[1408,512]{1,0:T(8,128)(2,1)S(1)} collective-permute-done((bf16[1408,512]{1,0:T(8,128)(2,1)}, bf16[1408,512]{1,0:T(8,128)(2,1)S(1)}, u32[]{:S(2)}, u32[]{:S(2)}) %collective-permute-start) | collective-permute-done | bytes 1441824 | tf_op jit(solution)/shard_map/ppermute | solution.py:18
  69.3 26.5 %collective-permute-start.2 = (bf16[1408,512]{1,0:T(8,128)(2,1)S(1)}, bf16[1408,512]{1,0:T(8,128)(2,1)}, u32[]{:S(2)}, u32[]{:S(2)}) collective-permute-start(bf16[1408,512]{1,0:T(8,128)(2,1)S(1)} %collective-permute-done), channel_id=1, source_target_pairs={{0,4},{4,8},{8,12},{12,0},{1,5},{5,9},{9,13},{13,1},{2,6},{6,10},{... | collective-permute-start | bytes 4325384 | tf_op jit(solution)/shard_map/ppermute | solution.py:18
  95.8 1.2 fusion.5
  97.1 3.2 broadcast.36.clone.1
  100.3 1.2 constant_dynamic-update-slice_fusion.7
  101.5 1.2 constant_dynamic-update-slice_fusion.6
  102.8 11.4 %collective-permute-done.1 = bf16[1408,512]{1,0:T(8,128)(2,1)} collective-permute-done((bf16[1408,512]{1,0:T(8,128)(2,1)}, bf16[1408,512]{1,0:T(8,128)(2,1)}, u32[]{:S(2)}, u32[]{:S(2)}) %collective-permute-start.1) | collective-permute-done | bytes 1441824 | tf_op jit(solution)/shard_map/ppermute | solution.py:23
  114.2 2.6 constant_dynamic-update-slice_fusion.5
  116.8 57.2 %collective-permute-done.2 = bf16[1408,512]{1,0:T(8,128)(2,1)} collective-permute-done((bf16[1408,512]{1,0:T(8,128)(2,1)S(1)}, bf16[1408,512]{1,0:T(8,128)(2,1)}, u32[]{:S(2)}, u32[]{:S(2)}) %collective-permute-start.2) | collective-permute-done | bytes 1441824 | tf_op jit(solution)/shard_map/ppermute | solution.py:18
  174.0 2.6 constant_dynamic-update-slice_fusion.4
  176.6 2.1 fusion.16
  178.7 55.9 %all-gather.6.cloned.1.call-done = bf16[2048,1408]{1,0:T(8,128)(2,1)} async-done(((bf16[512,1408]{1,0:T(8,128)(2,1)}), bf16[2048,1408]{1,0:T(8,128)(2,1)}) %all-gather.6.cloned.1.call-update) | async-done | bytes 5767184 | tf_op jit(solution)/shard_map/all_gather | solution.py:38
  234.6 4.5 fusion.12
  239.1 102.8 %all-gather.8.cloned.1.call-done = bf16[2048,1408]{1,0:T(8,128)(2,1)} async-done(((bf16[512,1408]{1,0:T(8,128)(2,1)}), bf16[2048,1408]{1,0:T(8,128)(2,1)}) %all-gather.8.cloned.1.call-update) | async-done | bytes 5767184 | tf_op jit(solution)/shard_map/all_gather | solution.py:39
  341.9 7.3 %fusion.1 = bf16[128,2048]{1,0:T(8,128)(2,1)} fusion(f32[128,2048]{1,0:T(8,128)S(1)} %fusion.16, bf16[1408,2048]{1,0:T(8,128)(2,1)} %constant_dynamic-update-slice_fusion.4, bf16[2048,1408]{1,0:T(8,128)(2,1)} %all-gather.8.cloned.1.call-done, f32[128,1408]{1,0:T(8,128)} %fusion.12, bf16[128,2048]{1,0:T(8,128)(2,1)S(1)} %copy-done.1, f32[2048]{0:T(1024)S(1)} %copy-done.5, ...), kind=kOutput, calls=%fused_computation.5 | convolution fusion | flops 1479311360 | bytes 14361088 | tf_op jit(solution)/shard_map/dot_general | solution.py:50
  349.2 0.0 all-gather.12.cloned.1.call-start
  349.3 0.5 all-gather.12.cloned.1.call-update
  349.8 0.0 all-gather.14.cloned.1.call-start
  349.9 0.5 all-gather.14.cloned.1.call-update
  350.5 0.1 collective-permute-start.3
  350.5 3.8 collective-permute-start.4
  354.3 35.2 %collective-permute-done.3 = bf16[1408,512]{1,0:T(8,128)(2,1)S(1)} collective-permute-done((bf16[1408,512]{1,0:T(8,128)(2,1)S(1)}, bf16[1408,512]{1,0:T(8,128)(2,1)S(1)}, u32[]{:S(2)}, u32[]{:S(2)}) %collective-permute-start.3) | collective-permute-done | bytes 1441824 | tf_op jit(solution)/shard_map/ppermute | solution.py:18
  389.5 3.2 broadcast.36.clone
  392.7 1.2 constant_dynamic-update-slice_fusion.3
  393.9 1.2 constant_dynamic-update-slice_fusion.2
  395.2 104.4 %collective-permute-done.4 = bf16[1408,512]{1,0:T(8,128)(2,1)} collective-permute-done((bf16[1408,512]{1,0:T(8,128)(2,1)S(1)}, bf16[1408,512]{1,0:T(8,128)(2,1)}, u32[]{:S(2)}, u32[]{:S(2)}) %collective-permute-start.4) | collective-permute-done | bytes 1441824 | tf_op jit(solution)/shard_map/ppermute | solution.py:23
  499.6 2.6 constant_dynamic-update-slice_fusion.1
  502.2 10.0 %collective-permute-done.5 = bf16[1408,512]{1,0:T(8,128)(2,1)} collective-permute-done((bf16[1408,512]{1,0:T(8,128)(2,1)S(1)}, bf16[1408,512]{1,0:T(8,128)(2,1)}, u32[]{:S(2)}, u32[]{:S(2)}) %collective-permute-start.5) | collective-permute-done | bytes 1441824 | tf_op jit(solution)/shard_map/ppermute | solution.py:18
  512.2 2.6 constant_dynamic-update-slice_fusion
  514.8 1.1 multiply_reduce_fusion
  515.9 1.0 multiply_convert_fusion
  516.9 7.1 %all_gather.24 = bf16[128,2048]{1,0:T(8,128)(2,1)S(1)} all-gather(bf16[32,2048]{1,0:T(8,128)(2,1)S(1)} %multiply_convert_fusion), channel_id=1, replica_groups=mesh['grp'=2,'fs'=4,'tp'=4] {'tp'}, dimensions={0}, use_global_device_ids=true | all-gather | bytes 655360 | tf_op jit(solution)/shard_map/all_gather | solution.py:62
  524.0 15.0 %all-gather.12.cloned.1.call-done = bf16[2048,1408]{1,0:T(8,128)(2,1)} async-done(((bf16[512,1408]{1,0:T(8,128)(2,1)}), bf16[2048,1408]{1,0:T(8,128)(2,1)}) %all-gather.12.cloned.1.call-update) | async-done | bytes 5767184 | tf_op jit(solution)/shard_map/all_gather | solution.py:38
  539.0 3.6 fusion.17
  542.7 104.4 %all-gather.14.cloned.1.call-done = bf16[2048,1408]{1,0:T(8,128)(2,1)} async-done(((bf16[512,1408]{1,0:T(8,128)(2,1)}), bf16[2048,1408]{1,0:T(8,128)(2,1)}) %all-gather.14.cloned.1.call-update) | async-done | bytes 5767184 | tf_op jit(solution)/shard_map/all_gather | solution.py:39
  647.0 7.1 %fusion.2 = bf16[128,2048]{1,0:T(8,128)(2,1)} fusion(bf16[1408,2048]{1,0:T(8,128)(2,1)} %constant_dynamic-update-slice_fusion, bf16[128,2048]{1,0:T(8,128)(2,1)S(1)} %all_gather.24, bf16[2048,1408]{1,0:T(8,128)(2,1)} %all-gather.14.cloned.1.call-done, f32[128,1408]{1,0:T(8,128)S(1)} %fusion.17), kind=kOutput, calls=%fused_computation.6 | convolution fusion | flops 1478000640 | bytes 13303808 | tf_op jit(solution)/shard_map/dot_general | solution.py:50
  654.1 20.0 %reduce-scatter.5.cloned.1.call-done = bf16[32,2048]{1,0:T(8,128)(2,1)} async-done(((bf16[128,2048]{1,0:T(8,128)(2,1)}), bf16[32,2048]{1,0:T(8,128)(2,1)}) %reduce-scatter.5.cloned.1.call-update) | async-done | bytes 131088 | tf_op jit(solution)/shard_map/reduce_scatter | solution.py:56
  674.2 1.0 add_convert_fusion
  675.1 6.6 all_gather.27
  681.7 0.8 copy.21
  (23 shorter events, 0.1 us)
Async XLA Ops:
  6.5 170.1 %copy-start = (bf16[128,512]{1,0:T(8,128)(2,1)S(1)}, bf16[128,512]{1,0:T(8,128)(2,1)}, u32[]{:S(2)}) copy-start(bf16[128,512]{1,0:T(8,128)(2,1)} %param.12) | copy-start | bytes 393220
  6.5 93.7 %copy-start.2 = (bf16[1408,512]{1,0:T(8,128)(2,1)S(1)}, bf16[1408,512]{1,0:T(8,128)(2,1)}, u32[]{:S(2)}) copy-start(bf16[1408,512]{1,0:T(8,128)(2,1)} %param.16) | copy-start | bytes 4325380
  6.5 170.1 %all-gather.10.cloned.1.call-start = ((), (), s32[]{:S(2)}) async-start(), calls=%async_computation.4 | async-start | bytes 2621440 | tf_op jit(solution)/shard_map/all_gather | solution.py:82
  7.3 227.3 %all-gather.6.cloned.1.call-start = ((), (), s32[]{:S(2)}) async-start(), calls=%async_computation.2 | async-start | bytes 7208960 | tf_op jit(solution)/shard_map/all_gather | solution.py:38
  8.0 333.9 %all-gather.8.cloned.1.call-start = ((), (), s32[]{:S(2)}) async-start(), calls=%async_computation.3 | async-start | bytes 7208960 | tf_op jit(solution)/shard_map/all_gather | solution.py:39
  8.7 506.1 %reduce-scatter.3.cloned.1.call-start = ((), (), s32[]{:S(2)}) async-start(), calls=%async_computation.5 | async-start | bytes 655360 | tf_op jit(solution)/shard_map/reduce_scatter | solution.py:56
  8.8 60.5 %collective-permute-start = (bf16[1408,512]{1,0:T(8,128)(2,1)}, bf16[1408,512]{1,0:T(8,128)(2,1)S(1)}, u32[]{:S(2)}, u32[]{:S(2)}) collective-permute-start(bf16[1408,512]{1,0:T(8,128)(2,1)} %param.16), channel_id=1, source_target_pairs={{0,4},{4,8},{8,12},{12,0},{1,5},{5,9},{9,13},{13,1},{2,6},{6,10},{... | collective-permute-start | bytes 4325384 | tf_op jit(solution)/shard_map/ppermute | solution.py:18
  11.9 102.3 %collective-permute-start.1 = (bf16[1408,512]{1,0:T(8,128)(2,1)}, bf16[1408,512]{1,0:T(8,128)(2,1)}, u32[]{:S(2)}, u32[]{:S(2)}) collective-permute-start(bf16[1408,512]{1,0:T(8,128)(2,1)} %param.16), channel_id=1, source_target_pairs={{0,12},{4,0},{8,4},{12,8},{1,13},{5,1},{9,5},{13,9},{2,14},{6,2},{... | collective-permute-start | bytes 4325384 | tf_op jit(solution)/shard_map/ppermute | solution.py:23
  69.3 104.7 %collective-permute-start.2 = (bf16[1408,512]{1,0:T(8,128)(2,1)S(1)}, bf16[1408,512]{1,0:T(8,128)(2,1)}, u32[]{:S(2)}, u32[]{:S(2)}) collective-permute-start(bf16[1408,512]{1,0:T(8,128)(2,1)S(1)} %collective-permute-done), channel_id=1, source_target_pairs={{0,4},{4,8},{8,12},{12,0},{1,5},{5,9},{9,13},{13,1},{2,6},{6,10},{... | collective-permute-start | bytes 4325384 | tf_op jit(solution)/shard_map/ppermute | solution.py:18
  101.5 133.1 %copy-start.1 = (bf16[128,2048]{1,0:T(8,128)(2,1)S(1)}, bf16[128,2048]{1,0:T(8,128)(2,1)}, u32[]{:S(2)}) copy-start(bf16[128,2048]{1,0:T(8,128)(2,1)} %param.11) | copy-start | bytes 1572868
  101.5 133.1 %copy-start.5 = (f32[2048]{0:T(1024)S(1)}, f32[2048]{0:T(1024)}, u32[]{:S(2)}) copy-start(f32[2048]{0:T(1024)} %param.13) | copy-start | bytes 24580
  239.1 111.3 %copy-start.3 = (bf16[1408,512]{1,0:T(8,128)(2,1)S(1)}, bf16[1408,512]{1,0:T(8,128)(2,1)}, u32[]{:S(2)}) copy-start(bf16[1408,512]{1,0:T(8,128)(2,1)} %param.21) | copy-start | bytes 4325380
  349.2 189.8 %all-gather.12.cloned.1.call-start = ((), (), s32[]{:S(2)}) async-start(), calls=%async_computation.6 | async-start | bytes 7208960 | tf_op jit(solution)/shard_map/all_gather | solution.py:38
  349.8 297.2 %all-gather.14.cloned.1.call-start = ((), (), s32[]{:S(2)}) async-start(), calls=%async_computation.7 | async-start | bytes 7208960 | tf_op jit(solution)/shard_map/all_gather | solution.py:39
  350.4 323.7 %reduce-scatter.5.cloned.1.call-start = ((), (), s32[]{:S(2)}) async-start(), calls=%async_computation.8 | async-start | bytes 655360 | tf_op jit(solution)/shard_map/reduce_scatter | solution.py:56
  350.5 39.1 %collective-permute-start.3 = (bf16[1408,512]{1,0:T(8,128)(2,1)S(1)}, bf16[1408,512]{1,0:T(8,128)(2,1)S(1)}, u32[]{:S(2)}, u32[]{:S(2)}) collective-permute-start(bf16[1408,512]{1,0:T(8,128)(2,1)S(1)} %copy-done.3), channel_id=1, source_target_pairs={{0,4},{4,8},{8,12},{12,0},{1,5},{5,9},{9,13},{13,1},{2,6},{6,10},{... | collective-permute-start | bytes 4325384 | tf_op jit(solution)/shard_map/ppermute | solution.py:18
  350.5 149.0 %collective-permute-start.4 = (bf16[1408,512]{1,0:T(8,128)(2,1)S(1)}, bf16[1408,512]{1,0:T(8,128)(2,1)}, u32[]{:S(2)}, u32[]{:S(2)}) collective-permute-start(bf16[1408,512]{1,0:T(8,128)(2,1)S(1)} %copy-done.3), channel_id=1, source_target_pairs={{0,12},{4,0},{8,4},{12,8},{1,13},{5,1},{9,5},{13,9},{2,14},{6,2},{... | collective-permute-start | bytes 4325384 | tf_op jit(solution)/shard_map/ppermute | solution.py:23
  389.5 122.7 %collective-permute-start.5 = (bf16[1408,512]{1,0:T(8,128)(2,1)S(1)}, bf16[1408,512]{1,0:T(8,128)(2,1)}, u32[]{:S(2)}, u32[]{:S(2)}) collective-permute-start(bf16[1408,512]{1,0:T(8,128)(2,1)S(1)} %collective-permute-done.3), channel_id=1, source_target_pairs={{0,4},{4,8},{8,12},{12,0},{1,5},{5,9},{9,13},{13,1},{2,6},{6,10},{... | collective-permute-start | bytes 4325384 | tf_op jit(solution)/shard_map/ppermute | solution.py:18
  392.7 123.2 %copy-start.6 = (f32[2048]{0:T(1024)S(1)}, f32[2048]{0:T(1024)}, u32[]{:S(2)}) copy-start(f32[2048]{0:T(1024)} %param.18) | copy-start | bytes 24580
  542.7 131.5 %copy-start.4 = (bf16[32,2048]{1,0:T(8,128)(2,1)S(1)}, bf16[32,2048]{1,0:T(8,128)(2,1)}, u32[]{:S(2)}) copy-start(bf16[32,2048]{1,0:T(8,128)(2,1)} %reduce-scatter.3.cloned.1.call-done) | copy-start | bytes 393220
Sparse Core Ops, SparseCore 0:
  8.9 87.7 all-gather.9
  98.3 136.2 all-gather.5
  236.1 105.7 all-gather.7
  349.4 19.8 reduce-scatter.2
  370.7 168.2 all-gather.11
  540.5 106.5 all-gather.13
  654.2 19.8 reduce-scatter.4
